TPU v7x, 32 devices: a whole 2x2x4 slice. The times are simulated.
32 devices in a mesh: sp: 4 (over y, x), tp: 8 (over z, core).
Axes of the slice: x: 2, y: 2, z: 4, core: 2. Of those that a mesh axis runs over, the one named last changes fastest.
Arguments:
- moe_input: bfloat16 [512, 2048], P('sp'), may hold values from -6 to 6
- cotangent: bfloat16 [512, 2048], P('sp'), may hold values from -6 to 6
- route_expert: int32 [512, 2], P('sp'), may hold values from 0 to 3, all different within a row; in each aligned block of 128 rows (0 to 127, 128 to 255, ...) at most 128 rows name the same one
- route_weight: float32 [512, 2], P('sp'), may hold values from 0.2 to 1
- w_gate: bfloat16 [4, 2048, 6144], P('sp', None, 'tp'), may hold values from -0.125 to 0.125
- w_up: bfloat16 [4, 2048, 6144], P('sp', None, 'tp'), may hold values from -0.125 to 0.125
- w_down: bfloat16 [4, 6144, 2048], P('sp', 'tp'), may hold values from -0.078125 to 0.078125
- out_proj: bfloat16 [2048, 2048], P('tp'), may hold values from -0.125 to 0.125
- saved_out: bfloat16 [512, 2048], P('sp', 'tp'), may hold values from -6 to 6
- queries: bfloat16 [512, 1024], P('sp', 'tp'), may hold values from -6 to 6
- keys: bfloat16 [512, 1024], P('sp', 'tp'), may hold values from -6 to 6
- values: bfloat16 [512, 2048], P('sp', 'tp'), may hold values from -6 to 6
- log_decay: float32 [512, 1024], P('sp', 'tp'), may hold values from -1 to 0
- span_state: float32 [8, 1024, 128], P('sp', 'tp'), may hold values from -6 to 6
Outputs:
- grad_w_gate: bfloat16 [4, 2048, 6144], P('sp', None, 'tp')
- grad_w_up: bfloat16 [4, 2048, 6144], P('sp', None, 'tp')
- grad_w_down: bfloat16 [4, 6144, 2048], P('sp', 'tp')
- grad_proj: float32 [2048, 2048], P('sp', 'tp')
- grad_queries: bfloat16 [512, 1024], P('sp', 'tp')
- grad_keys: bfloat16 [512, 1024], P('sp', 'tp')
- grad_values: bfloat16 [512, 2048], P('sp', 'tp')
- grad_decay: float32 [512, 1024], P('sp', 'tp')
Inputs may be any that keep to these rules, and one draw needn't show every extreme that they name: `route_expert`: each row names two different experts. Within the 128 rows of one index of sp no expert is named by more than 128 rows, a bound that some block reaches.
All inputs are finite; a program needn't handle non-finite values.
Results may differ from a plain program's by a relative error of at most 0.019.
Values may be sent and summed in bfloat16 or wider, within the bound.
No kernel may reach another device: no remote copies, remote signals or barrier semaphores. Data moves between devices by JAX's collectives and lax.ppermute only.
A program may use at most 128 MiB of HBM per device.

v0:
```python
import jax
import jax.numpy as jnp
from jax import lax
from jax.sharding import PartitionSpec as P

DK = 64
SPAN = 64
HIGH = lax.Precision.HIGHEST


def entering(shard, axis, combine, identity):
    length, mine = (lax.axis_size(axis), lax.axis_index(axis))
    everything = jax.tree.map(lambda part: lax.all_gather(part, axis), shard)
    start = jax.tree.map(
        lambda part, zero: jnp.broadcast_to(jnp.asarray(zero, part.dtype), part.shape),
        shard,
        identity,
    )

    def step(k, before):
        at = length - 1 - k
        reached = at > mine
        new = combine(before, jax.tree.map(lambda part: part[at], everything))
        return jax.tree.map(lambda a, b: jnp.where(reached, a, b), new, before)

    return lax.fori_loop(0, length, step, start)


def slot_places(experts, count):
    routes_flat = experts.reshape(-1)
    one_hot = (routes_flat[:, None] == jnp.arange(count, dtype=jnp.int32)[None, :]).astype(
        jnp.int32
    )
    earlier = jnp.cumsum(one_hot, axis=0) - one_hot
    return jnp.sum(earlier * one_hot, axis=1).reshape(experts.shape)


def expert_grads(inputs, routed, gate_weight, up_weight, down_weight):
    gate = jnp.dot(inputs, gate_weight, preferred_element_type=jnp.float32)
    upper = jnp.dot(inputs, up_weight, preferred_element_type=jnp.float32)
    sigmoid_gate = jax.nn.sigmoid(gate)
    active = gate * sigmoid_gate
    hidden = (active * upper).astype(jnp.bfloat16)
    d_hidden = lax.dot_general(
        routed, down_weight, (((1,), (1,)), ((), ())), preferred_element_type=jnp.float32
    )
    d_upper = (d_hidden * active).astype(jnp.bfloat16)
    d_gate = (d_hidden * upper * sigmoid_gate * (1.0 + gate * (1.0 - sigmoid_gate))).astype(
        jnp.bfloat16
    )
    grad_down = lax.dot_general(
        hidden, routed, (((0,), (0,)), ((), ())), preferred_element_type=jnp.float32
    ).astype(jnp.bfloat16)
    grad_gate = lax.dot_general(
        inputs, d_gate, (((0,), (0,)), ((), ())), preferred_element_type=jnp.float32
    ).astype(jnp.bfloat16)
    grad_up = lax.dot_general(
        inputs, d_upper, (((0,), (0,)), ((), ())), preferred_element_type=jnp.float32
    ).astype(jnp.bfloat16)
    return (d_gate, d_upper, grad_gate, grad_up, grad_down)


def input_grad(d_gate, d_upper, gate_weight, up_weight):
    first = lax.dot_general(
        d_gate, gate_weight, (((1,), (1,)), ((), ())), preferred_element_type=jnp.float32
    )
    second = lax.dot_general(
        d_upper, up_weight, (((1,), (1,)), ((), ())), preferred_element_type=jnp.float32
    )
    return first + second


def gated_pieces(queries, keys, values, log_decay, grad_mix, key_dim, span_len):
    value_dim = values.shape[1] * key_dim // queries.shape[1]
    heads = queries.shape[1] // key_dim
    spans = queries.shape[0] // span_len

    def blocks(array, width):
        return array.astype(jnp.float32).reshape(spans, span_len, heads, width)

    query_spans = blocks(queries, key_dim)
    key_spans = blocks(keys, key_dim)
    value_spans = blocks(values, value_dim)
    grad_spans = blocks(grad_mix, value_dim)
    cumulative = jnp.cumsum(blocks(log_decay, key_dim), axis=1)
    last = cumulative[:, -1]
    scale = key_dim ** (-0.5)
    query_decayed = query_spans * jnp.exp(cumulative)
    key_grown = key_spans * jnp.exp(-cumulative)
    key_to_end = key_spans * jnp.exp(last[:, None] - cumulative)
    g_local = scale * jnp.einsum("nthk,nthv->nhkv", query_decayed, grad_spans, precision=HIGH)
    return (
        query_spans,
        key_spans,
        value_spans,
        grad_spans,
        cumulative,
        last,
        query_decayed,
        key_grown,
        key_to_end,
        g_local,
    )


def backward_step(carry, inputs):
    local, decay = inputs
    return (local + jnp.exp(decay)[..., None] * carry, carry)


def gated_finish(pieces, span_state, g_end, key_dim):
    (
        query_spans,
        key_spans,
        value_spans,
        grad_spans,
        cumulative,
        last,
        query_decayed,
        key_grown,
        key_to_end,
        g_local,
    ) = pieces
    spans, span_len, heads, value_dim = value_spans.shape
    scale = key_dim ** (-0.5)
    token_locations = jnp.arange(span_len, dtype=jnp.int32)
    causal = (token_locations[:, None] >= token_locations[None, :]).astype(jnp.float32)
    scores = jnp.einsum("nthk,nshk->nhts", query_decayed, key_grown, precision=HIGH) * causal
    grad_dot = jnp.einsum("nthv,nshv->nhts", grad_spans, value_spans, precision=HIGH) * causal
    state = span_state.reshape(spans, heads, key_dim, value_dim)
    d_query = (
        scale
        * jnp.exp(cumulative)
        * (
            jnp.einsum("nhts,nshk->nthk", grad_dot, key_grown, precision=HIGH)
            + jnp.einsum("nthv,nhkv->nthk", grad_spans, state, precision=HIGH)
        )
    )
    d_key = scale * jnp.exp(-cumulative) * jnp.einsum(
        "nhts,nthk->nshk", grad_dot, query_decayed, precision=HIGH
    ) + jnp.exp(last[:, None] - cumulative) * jnp.einsum(
        "nshv,nhkv->nshk", value_spans, g_end, precision=HIGH
    )
    d_value = scale * jnp.einsum(
        "nhts,nthv->nshv", scores, grad_spans, precision=HIGH
    ) + jnp.einsum("nshk,nhkv->nshv", key_to_end, g_end, precision=HIGH)
    state_end = jnp.exp(last)[..., None] * state + jnp.einsum(
        "nshk,nshv->nhkv", key_to_end, value_spans, precision=HIGH
    )
    tail = jnp.sum(state_end * g_end, axis=-1)
    d_cumulative = query_spans * d_query - key_spans * d_key
    d_log = jnp.cumsum(d_cumulative[:, ::-1], axis=1)[:, ::-1] + tail[:, None]
    rows = spans * span_len
    return (
        d_query.reshape(rows, heads * key_dim).astype(jnp.bfloat16),
        d_key.reshape(rows, heads * key_dim).astype(jnp.bfloat16),
        d_value.reshape(rows, heads * value_dim).astype(jnp.bfloat16),
        d_log.reshape(rows, heads * key_dim),
    )


def carry_combine(earlier, later):
    return (later[0] * earlier[0], later[1] + later[0][..., None] * earlier[1])


def on_device(
    moe_input,
    cotangent,
    route_expert,
    route_weight,
    w_gate,
    w_up,
    w_down,
    out_proj,
    saved_out,
    queries,
    keys,
    values,
    log_decay,
    span_state,
):
    tok_rows, width = moe_input.shape
    groups = lax.axis_size("sp")
    lanes = lax.axis_size("tp")
    capacity = 4 * tok_rows // groups
    target_locations = slot_places(route_expert, groups)
    rows_index = (target_locations * groups + route_expert).reshape(-1)
    owner = (
        jnp.full((capacity * groups,), 2 * tok_rows, jnp.int32)
        .at[rows_index]
        .set(jnp.arange(2 * tok_rows, dtype=jnp.int32))
    )
    weighted = (route_weight[:, :, None] * cotangent[:, None, :].astype(jnp.float32)).astype(
        jnp.bfloat16
    )
    weighted = weighted.reshape(2 * tok_rows, width)
    blank = jnp.zeros((1, width), jnp.bfloat16)
    send_in = jnp.concatenate([moe_input, blank], axis=0)[owner // 2].reshape(
        capacity, groups, width
    )
    send_cot = jnp.concatenate([weighted, blank], axis=0)[owner].reshape(capacity, groups, width)
    gate_weight = w_gate[0]
    up_weight = w_up[0]
    down_weight = w_down[0]
    share = capacity // lanes
    lane = lax.axis_index("tp")
    part_in = lax.dynamic_slice_in_dim(send_in, lane * share, share, 0)
    part_cot = lax.dynamic_slice_in_dim(send_cot, lane * share, share, 0)
    got_in, got_cot = (
        lax.all_to_all(part_in, "sp", split_axis=1, concat_axis=1, tiled=True),
        lax.all_to_all(part_cot, "sp", split_axis=1, concat_axis=1, tiled=True),
    )
    full_in, full_cot = (
        lax.all_gather(got_in, "tp", axis=0, tiled=True),
        lax.all_gather(got_cot, "tp", axis=0, tiled=True),
    )
    d_gate, d_upper, grad_gate, grad_up, grad_down = expert_grads(
        full_in.reshape(-1, width), full_cot.reshape(-1, width), gate_weight, up_weight, down_weight
    )
    mine = (
        lax.psum_scatter(
            input_grad(d_gate, d_upper, gate_weight, up_weight).astype(jnp.bfloat16),
            "tp",
            scatter_dimension=0,
            tiled=True,
        )
        .astype(jnp.float32)
        .reshape(share, groups, width)
    )
    returned = (
        lax.all_to_all(mine.astype(jnp.bfloat16), "sp", split_axis=1, concat_axis=1, tiled=True)
        .astype(mine.dtype)
        .reshape(-1, width)
    )
    local_index = rows_index - lane * share * groups
    inside = (local_index >= 0) & (local_index < share * groups)
    picked = jnp.where(inside[:, None], returned[jnp.clip(local_index, 0, share * groups - 1)], 0.0)
    routed = jnp.sum(picked.reshape(tok_rows, 2, width), axis=1)
    total = lax.psum(routed.astype(jnp.bfloat16), "tp").astype(jnp.float32)
    grad_in = (cotangent.astype(jnp.float32) + total).astype(jnp.bfloat16)
    grad_mix = lax.dot_general(
        grad_in, out_proj, (((1,), (1,)), ((), ())), preferred_element_type=jnp.float32
    )
    grad_proj = lax.psum_scatter(
        lax.dot_general(
            grad_in, saved_out, (((0,), (0,)), ((), ())), preferred_element_type=jnp.float32
        ).astype(jnp.bfloat16),
        "sp",
        scatter_dimension=0,
        tiled=True,
    ).astype(jnp.float32)
    pieces = gated_pieces(queries, keys, values, log_decay, grad_mix, DK, SPAN)
    g_local = pieces[9]
    last = pieces[5]
    begin = jnp.zeros(g_local.shape[1:], jnp.float32)
    device_start, local_end = lax.scan(backward_step, begin, (g_local, last), reverse=True)
    device_decay = jnp.exp(jnp.sum(last, axis=0))
    identity = (jnp.ones_like(device_decay), jnp.zeros_like(device_start))
    decay_after, state_after = entering((device_decay, device_start), "sp", carry_combine, identity)
    running = jnp.cumsum(last, axis=0)
    beyond = running[-1][None] - running
    g_end = local_end + jnp.exp(beyond)[..., None] * state_after[None]
    grad_queries, grad_keys, grad_values, grad_decay = gated_finish(pieces, span_state, g_end, DK)
    return (
        grad_gate[None],
        grad_up[None],
        grad_down[None],
        grad_proj,
        grad_queries,
        grad_keys,
        grad_values,
        grad_decay,
    )


def solution(mesh):
    placed = (
        P("sp", None),
        P("sp", None),
        P("sp", None),
        P("sp", None),
        P("sp", None, "tp"),
        P("sp", None, "tp"),
        P("sp", "tp", None),
        P("tp", None),
        P("sp", "tp"),
        P("sp", "tp"),
        P("sp", "tp"),
        P("sp", "tp"),
        P("sp", "tp"),
        P("sp", "tp", None),
    )
    return jax.shard_map(
        on_device,
        mesh=mesh,
        in_specs=placed,
        out_specs=(
            P("sp", None, "tp"),
            P("sp", None, "tp"),
            P("sp", "tp", None),
            P("sp", "tp"),
            P("sp", "tp"),
            P("sp", "tp"),
            P("sp", "tp"),
            P("sp", "tp"),
        ),
        check_vma=False,
    )
```

profile of v0, /device:TPU:0, one launch (start us, length us, event | category | flops | bytes accessed | tf_op | source)
XLA Modules:
  0.0 273.4 jit_solution(1842844893253880070)
XLA Ops:
  8.5 1.2 reduce-window.6
  11.3 1.4 scatter_custom_fusion
  12.7 1.9 concatenate.6
  14.6 6.3 %gather_fusion = bf16[512,2048]{1,0:T(8,128)(2,1)} fusion(bf16[129,2048]{1,0:T(8,128)(2,1)} %concatenate.6, s32[1024]{0:T(1024)S(1)} %get-tuple-element.318), kind=kCustom, calls=%fused_computation | custom fusion | bytes 4196352 | tf_op jit(solution)/shard_map/gather | solution.py:198
  21.0 4.1 %reshape.208 = bf16[128,4,2048]{2,1,0:T(4,128)(2,1)} reshape(bf16[512,2048]{1,0:T(8,128)(2,1)} %gather_fusion) | data formatting | bytes 4194304 | tf_op jit(solution)/shard_map/reshape | solution.py:198
  25.1 1.0 constant_dynamic-slice_fusion.1
  26.3 10.7 %all_to_all.15 = bf16[16,4,2048]{2,0,1:T(8,128)(2,1)S(1)} all-to-all(bf16[16,4,2048]{2,0,1:T(8,128)(2,1)S(1)} %copy.146), channel_id=1, replica_groups=mesh['sp'=4,'tp'=8] {'sp'}, dimensions={1} | all-to-all | bytes 524288 | tf_op jit(solution)/shard_map/all_to_all | solution.py:210
  38.0 3.4 %mul.203 = f32[128,2,2048]{2,1,0:T(2,128)} broadcast(bf16[128,2048]{1,0:T(8,128)(2,1)} %param.19), dimensions={0,2} | broadcast | bytes 2621440 | tf_op jit(solution)/shard_map/mul | solution.py:193
  41.4 3.7 %mul.204 = f32[256,2048]{1,0:T(8,128)} reshape(f32[128,2,2048]{2,1,0:T(2,128)} %mul.203) | data formatting | bytes 4194304 | tf_op jit(solution)/shard_map/mul | solution.py:193
  45.3 1.9 multiply_convert_fusion
  47.2 1.1 concatenate.7
  48.3 6.6 %gather_fusion.1 = bf16[512,2048]{1,0:T(8,128)(2,1)} fusion(bf16[257,2048]{1,0:T(8,128)(2,1)} %concatenate.7, s32[1024]{0:T(1024)S(1)} %get-tuple-element.317), kind=kCustom, calls=%fused_computation.1 | custom fusion | bytes 4196352 | tf_op jit(solution)/shard_map/gather | solution.py:201
  54.9 4.1 %reshape.210 = bf16[128,4,2048]{2,1,0:T(4,128)(2,1)} reshape(bf16[512,2048]{1,0:T(8,128)(2,1)} %gather_fusion.1) | data formatting | bytes 4194304 | tf_op jit(solution)/shard_map/reshape | solution.py:201
  59.0 1.0 constant_dynamic-slice_fusion
  60.2 8.1 %all_to_all.16 = bf16[16,4,2048]{2,0,1:T(8,128)(2,1)S(1)} all-to-all(bf16[16,4,2048]{2,0,1:T(8,128)(2,1)S(1)} %copy.147), channel_id=1, replica_groups=mesh['sp'=4,'tp'=8] {'sp'}, dimensions={1} | all-to-all | bytes 524288 | tf_op jit(solution)/shard_map/all_to_all | solution.py:211
  69.5 3.9 %reshape.209 = bf16[512,2048]{1,0:T(8,128)(2,1)} reshape(bf16[128,4,2048]{2,1,0:T(4,128)(2,1)} %all-gather.6.cloned.1.call-done) | data formatting | bytes 4194304 | tf_op jit(solution)/shard_map/reshape | solution.py:218
  73.5 4.7 %fusion.3 = f32[512,768]{1,0:T(8,128)} fusion(bf16[512,2048]{1,0:T(8,128)(2,1)} %reshape.209, bf16[1,2048,768]{2,1,0:T(8,128)(2,1)S(1)} %copy-done), kind=kOutput, calls=%fused_computation.16 | convolution fusion | flops 1610612736 | bytes 6815744 | tf_op jit(solution)/shard_map/dot_general | solution.py:39
  78.2 2.9 %fusion.7 = f32[512,768]{1,0:T(8,128)} fusion(bf16[512,2048]{1,0:T(8,128)(2,1)S(1)} %copy-done.4, bf16[1,2048,768]{2,1,0:T(8,128)(2,1)S(1)} %copy-done.17), kind=kOutput, calls=%fused_computation.20 | convolution fusion | flops 1610612736 | bytes 6815744 | tf_op jit(solution)/shard_map/dot_general | solution.py:40
  81.1 17.2 %all-gather.8.cloned.1.call-done = bf16[128,4,2048]{2,1,0:T(4,128)(2,1)} async-done(((bf16[16,4,2048]{2,1,0:T(4,128)(2,1)}), bf16[128,4,2048]{2,1,0:T(4,128)(2,1)}) %all-gather.8.cloned.1.call-update) | async-done | bytes 2097168 | tf_op jit(solution)/shard_map/all_gather | solution.py:215
  98.3 3.9 %reshape.211 = bf16[512,2048]{1,0:T(8,128)(2,1)} reshape(bf16[128,4,2048]{2,1,0:T(4,128)(2,1)} %all-gather.8.cloned.1.call-done) | data formatting | bytes 4194304 | tf_op jit(solution)/shard_map/reshape | solution.py:218
  102.3 5.6 %multiply_convert_fusion.2 = (bf16[512,768]{1,0:T(8,128)(2,1)S(1)}, bf16[512,768]{1,0:T(8,128)(2,1)S(1)}) fusion(f32[512,768]{1,0:T(8,128)} %fusion.3, f32[512,768]{1,0:T(8,128)} %fusion.7, bf16[512,2048]{1,0:T(8,128)(2,1)} %reshape.211, bf16[1,768,2048]{2,1,0:T(8,128)(2,1)} %param.24), kind=kOutput, calls=%fused_computation.31 | convolution fusion | flops 1615724544 | bytes 9961472 | tf_op jit(solution)/shard_map/dot_general | solution.py:44
  107.9 1.8 fusion.1
  110.4 3.2 %add_convert_fusion = bf16[512,2048]{1,0:T(8,128)(2,1)} fusion(f32[512,2048]{1,0:T(8,128)S(1)} %fusion.1, bf16[512,768]{1,0:T(8,128)(2,1)S(1)} %get-tuple-element.305, bf16[1,2048,768]{2,1,0:T(8,128)(2,1)S(1)} %copy-done.18), kind=kOutput, calls=%fused_computation.10 | convolution fusion | flops 1612709888 | bytes 10223616 | tf_op jit(solution)/shard_map/dot_general | solution.py:67
  115.3 8.0 %all-gather.2 = f32[4,2,64]{2,1,0:T(2,128)S(1)} all-gather(f32[1,2,64]{2,1,0:T(2,128)S(1)} %exponential_bitcast_fusion.1), channel_id=3, replica_groups=mesh['sp'=4,'tp'=8] {'sp'}, dimensions={0}, use_global_device_ids=true | all-gather | bytes 2560 | tf_op jit(solution)/shard_map/all_gather | solution.py:13
  123.4 1.1 convolution_multiply_fusion.2
  124.4 6.3 %fusion.13 = bf16[1,768,2048]{2,1,0:T(8,128)(2,1)} fusion(bf16[512,2048]{1,0:T(8,128)(2,1)} %reshape.211, f32[512,768]{1,0:T(8,128)} %fusion.7, f32[512,768]{1,0:T(8,128)} %fusion.3), kind=kOutput, calls=%fused_computation.26 | convolution fusion | flops 1614544896 | bytes 8388608 | tf_op jit(solution)/shard_map/dot_general | solution.py:51
  130.7 18.3 %reduce-scatter.3.cloned.1.call-done = bf16[64,2048]{1,0:T(8,128)(2,1)} async-done(((bf16[512,2048]{1,0:T(8,128)(2,1)}), bf16[64,2048]{1,0:T(8,128)(2,1)}) %reduce-scatter.3.cloned.1.call-update) | async-done | bytes 262160 | tf_op jit(solution)/shard_map/reduce_scatter | solution.py:221
  149.0 1.1 convert_element_type.102
  150.9 3.8 %all-to-all-start.2 = ((bf16[16,4,2048]{2,0,1:T(8,128)(2,1)}), bf16[16,4,2048]{2,0,1:T(8,128)(2,1)S(1)}, u32[]{:S(2)}, u32[]{:S(2)}) async-start(bf16[16,4,2048]{2,0,1:T(8,128)(2,1)} %copy.115), calls=%async_computation.3 | async-start | bytes 524288 | tf_op jit(solution)/shard_map/all_to_all | solution.py:231
  154.7 4.6 %fusion.12 = bf16[1,2048,768]{2,1,0:T(8,128)(2,1)} fusion(bf16[512,2048]{1,0:T(8,128)(2,1)S(1)} %copy-done.5, bf16[512,768]{1,0:T(8,128)(2,1)} %copy-done.19), kind=kOutput, calls=%fused_computation.25 | convolution fusion | flops 1612185600 | bytes 6029312 | tf_op jit(solution)/shard_map/dot_general | solution.py:57
  160.5 1.5 gather_fusion.2
  161.9 2.3 gather.14
  164.2 5.8 %select_reduce_fusion = bf16[128,2048]{1,0:T(8,128)(2,1)} fusion(f32[128,2,2048]{2,1,0:T(2,128)} %gather.14, pred[128,2]{1,0:T(8,128)(4,1)S(1)} %copy.114), kind=kLoop, calls=%fused_computation.28 | loop fusion | flops 786432 | bytes 2621696 | tf_op jit(solution)/shard_map/reduce_sum | solution.py:238
  170.2 4.7 %fusion.11 = bf16[1,2048,768]{2,1,0:T(8,128)(2,1)} fusion(bf16[512,2048]{1,0:T(8,128)(2,1)S(1)} %copy-done.6, bf16[512,768]{1,0:T(8,128)(2,1)} %copy-done.20), kind=kOutput, calls=%fused_computation.24 | convolution fusion | flops 1612185600 | bytes 6029312 | tf_op jit(solution)/shard_map/dot_general | solution.py:54
  174.9 49.9 %all-reduce.4.cloned.1.call-done = bf16[128,2048]{1,0:T(8,128)(2,1)} async-done(((bf16[128,2048]{1,0:T(8,128)(2,1)}), bf16[128,2048]{1,0:T(8,128)(2,1)}) %all-reduce.4.cloned.1.call-update) | async-done | bytes 524304 | tf_op jit(solution)/shard_map/psum | solution.py:239
  224.7 1.9 fusion.27
  227.4 9.5 %all-gather = f32[8,64,128]{2,1,0:T(8,128)S(1)} all-gather(f32[2,64,128]{2,1,0:T(8,128)S(1)} %get-tuple-element.245), channel_id=2, replica_groups=mesh['sp'=4,'tp'=8] {'sp'}, dimensions={0}, use_global_device_ids=true | all-gather | bytes 327680 | tf_op jit(solution)/shard_map/all_gather | solution.py:13
  237.5 1.4 convolution_convert_fusion.3
  240.2 1.0 multiply_subtract_fusion
  241.2 1.8 rev.6
  243.0 1.7 copy.139
  244.7 1.3 fusion.24
  246.1 1.0 fusion.57
  247.8 1.7 reshape.222
  249.4 1.4 convolution_multiply_fusion.1
  250.8 1.4 fusion.25
  255.4 9.7 %reduce-scatter.5.cloned.1.call-done = bf16[512,256]{1,0:T(8,128)(2,1)} async-done(((bf16[2048,256]{1,0:T(8,128)(2,1)}), bf16[512,256]{1,0:T(8,128)(2,1)}) %reduce-scatter.5.cloned.1.call-update) | async-done | bytes 262160 | tf_op jit(solution)/shard_map/reduce_scatter | solution.py:244
  265.1 1.8 convert_element_type.107
  (133 shorter events, 16.9 us)
Async XLA Ops:
  7.2 66.3 %copy-start = (bf16[1,2048,768]{2,1,0:T(8,128)(2,1)S(1)}, bf16[1,2048,768]{2,1,0:T(8,128)(2,1)}, u32[]{:S(2)}) copy-start(bf16[1,2048,768]{2,1,0:T(8,128)(2,1)} %param.22) | copy-start | bytes 9437188
  7.2 62.3 %all-gather.6.cloned.1.call-start = ((), (), s32[]{:S(2)}) async-start(), calls=%async_computation.5 | async-start | bytes 2359296 | tf_op jit(solution)/shard_map/all_gather | solution.py:214
  38.0 60.4 %all-gather.8.cloned.1.call-start = ((), (), s32[]{:S(2)}) async-start(), calls=%async_computation.6 | async-start | bytes 2359296 | tf_op jit(solution)/shard_map/all_gather | solution.py:215
  41.4 3.7 %copy-start.16 = (f32[128,2]{0,1:T(2,128)S(1)}, f32[128,2]{0,1:T(2,128)}, u32[]{:S(2)}) copy-start(f32[128,2]{0,1:T(2,128)} %param.21) | copy-start | bytes 3076
  69.3 79.7 %reduce-scatter.3.cloned.1.call-start = ((), (), s32[]{:S(2)}) async-start(), calls=%async_computation.7 | async-start | bytes 2359296 | tf_op jit(solution)/shard_map/reduce_scatter | solution.py:221
  73.5 4.7 %copy-start.4 = (bf16[512,2048]{1,0:T(8,128)(2,1)S(1)}, bf16[512,2048]{1,0:T(8,128)(2,1)}, u32[]{:S(2)}) copy-start(bf16[512,2048]{1,0:T(8,128)(2,1)} %reshape.209) | copy-start | bytes 6291460
  73.5 4.7 %copy-start.17 = (bf16[1,2048,768]{2,1,0:T(8,128)(2,1)S(1)}, bf16[1,2048,768]{2,1,0:T(8,128)(2,1)}, u32[]{:S(2)}) copy-start(bf16[1,2048,768]{2,1,0:T(8,128)(2,1)} %param.23) | copy-start | bytes 9437188
  107.9 1.9 copy-start.20
  107.9 1.9 copy-start.19
  107.9 2.5 copy-start.18
  113.6 0.8 copy-start.11
  113.6 1.2 copy-start.14
  113.6 1.4 copy-start.15
  113.6 1.7 copy-start.13
  124.4 30.3 %copy-start.5 = (bf16[512,2048]{1,0:T(8,128)(2,1)S(1)}, bf16[512,2048]{1,0:T(8,128)(2,1)}, u32[]{:S(2)}) copy-start(bf16[512,2048]{1,0:T(8,128)(2,1)} %reshape.209) | copy-start | bytes 6291460
  150.9 9.2 %all-to-all-start.2 = ((bf16[16,4,2048]{2,0,1:T(8,128)(2,1)}), bf16[16,4,2048]{2,0,1:T(8,128)(2,1)S(1)}, u32[]{:S(2)}, u32[]{:S(2)}) async-start(bf16[16,4,2048]{2,0,1:T(8,128)(2,1)} %copy.115), calls=%async_computation.3 | async-start | bytes 524288 | tf_op jit(solution)/shard_map/all_to_all | solution.py:231
  154.7 70.0 %all-reduce.4.cloned.1.call-start = ((), (), s32[]{:S(2)}) async-start(), calls=%async_computation.8 | async-start | bytes 1048576 | tf_op jit(solution)/shard_map/psum | solution.py:239
  164.2 5.9 %copy-start.6 = (bf16[512,2048]{1,0:T(8,128)(2,1)S(1)}, bf16[512,2048]{1,0:T(8,128)(2,1)}, u32[]{:S(2)}) copy-start(bf16[512,2048]{1,0:T(8,128)(2,1)} %reshape.209) | copy-start | bytes 6291460
  170.1 54.6 %copy-start.2 = (bf16[128,2048]{1,0:T(8,128)(2,1)S(1)}, bf16[128,2048]{1,0:T(8,128)(2,1)}, u32[]{:S(2)}) copy-start(bf16[128,2048]{1,0:T(8,128)(2,1)} %param.19) | copy-start | bytes 1572868
  170.1 95.0 %reduce-scatter.5.cloned.1.call-start = ((), (), s32[]{:S(2)}) async-start(), calls=%async_computation.9 | async-start | bytes 1310720 | tf_op jit(solution)/shard_map/reduce_scatter | solution.py:244
  226.6 10.8 %copy-start.7 = (bf16[128,2048]{1,0:T(8,128)(2,1)S(1)}, bf16[128,2048]{1,0:T(8,128)(2,1)}, u32[]{:S(2)}) copy-start(bf16[128,2048]{1,0:T(8,128)(2,1)} %all-reduce.4.cloned.1.call-done) | copy-start | bytes 1572868
  226.6 10.8 %copy-start.12 = (bf16[128,256]{1,0:T(8,128)(2,1)S(1)}, bf16[128,256]{1,0:T(8,128)(2,1)}, u32[]{:S(2)}) copy-start(bf16[128,256]{1,0:T(8,128)(2,1)} %param.26) | copy-start | bytes 196612
  226.7 12.5 %copy-start.3 = (f32[2,64,2,128]{3,2,1,0:T(2,128)}, f32[2,64,2,128]{3,2,1,0:T(2,128)S(1)}, u32[]{:S(2)}) copy-start(f32[2,64,2,128]{3,2,1,0:T(2,128)S(1)} %reshape.217) | copy-start | bytes 393220
  227.4 12.2 %copy-start.8 = (f32[2,2,64,128]{3,2,1,0:T(8,128)}, f32[2,2,64,128]{3,2,1,0:T(8,128)S(1)}, u32[]{:S(2)}) copy-start(f32[2,2,64,128]{3,2,1,0:T(8,128)S(1)} %get-tuple-element.244) | copy-start | bytes 393220
  237.5 1.7 copy-start.9
  241.2 25.7 %copy-start.1 = (bf16[1,2048,768]{2,1,0:T(8,128)(2,1)S(1)}, bf16[1,2048,768]{2,1,0:T(8,128)(2,1)}, u32[]{:S(2)}) copy-start(bf16[1,2048,768]{2,1,0:T(8,128)(2,1)} %param.22) | copy-start | bytes 9437188
  246.1 8.5 %copy-start.10 = (bf16[2,64,2,64]{1,3,2,0:T(8,128)(2,1)S(1)}, bf16[2,64,2,64]{1,3,2,0:T(8,128)(2,1)}, u32[]{:S(2)}) copy-start(bf16[2,64,2,64]{1,3,2,0:T(8,128)(2,1)} %get-tuple-element.309) | copy-start | bytes 98308
Sparse Core Ops, SparseCore 0:
  38.1 28.8 all-gather.5
  69.4 28.8 all-gather.7
  113.7 35.2 reduce-scatter.2
  170.2 54.4 all-reduce.3
  239.1 26.0 reduce-scatter.4
where the time goes:
time: 275 us; the launch traced here: 273 us
  waiting for transfers between devices  95.9 us (35%)
  local copies, waits for them, and re-layouts  63.6 us (23%)
  matrix products  44.8 us (16%)
  blocking collectives  36.4 us (13%)
  between operations  14.4 us (5%)
  other arithmetic  14 us (5%)
  starting transfers between devices  4.16 us (2%)
    psum x1, waiting for transfers between devices, on_device(): total = lax.psum(routed.astype(jnp.bfloat16), 'tp').astype(jnp.float32)  49.9 us
    reduce_scatter x1, waiting for transfers between devices, on_device(): lax.psum_scatter(input_grad(d_gate, d_upper, gate_weight, up_weight).asty...  18.3 us
    all_gather x2, blocking collectives, entering(): everything = jax.tree.map(lambda part: lax.all_gather(part, axis), shard)  17.5 us
    all_gather x1, waiting for transfers between devices, on_device(): lax.all_gather(got_cot, 'tp', axis=0, tiled=True)  17.2 us
    all_to_all x1, blocking collectives, on_device(): lax.all_to_all(part_in, 'sp', split_axis=1, concat_axis=1, tiled=True)  10.7 us
    reduce_scatter x1, waiting for transfers between devices, on_device(): lax.psum_scatter(lax.dot_general(grad_in, saved_out, (((0,), (0,)), ((),...  9.71 us
    all_to_all x1, blocking collectives, on_device(): lax.all_to_all(part_cot, 'sp', split_axis=1, concat_axis=1, tiled=True)  8.11 us
    mul x3, local copies, waits for them, and re-layouts, on_device(): route_weight[:, :, None] * cotangent[:, None, :].astype(jnp.float32)  7.21 us
  transfers between devices with their start and end apart: 6, of which 5 were waited for; matrix products, arithmetic and copies ran while one was open for 25% of the time, Pallas kernels for 0%

commit v1 on v0

--- a/solution.py
+++ b/solution.py
@@ -236,7 +236,7 @@
     inside = (local_index >= 0) & (local_index < share * groups)
     picked = jnp.where(inside[:, None], returned[jnp.clip(local_index, 0, share * groups - 1)], 0.0)
     routed = jnp.sum(picked.reshape(tok_rows, 2, width), axis=1)
-    total = lax.psum(routed.astype(jnp.bfloat16), "tp").astype(jnp.float32)
+    total = jnp.sum(lax.all_gather(routed.astype(jnp.bfloat16), "tp"), axis=0).astype(jnp.float32)
     grad_in = (cotangent.astype(jnp.float32) + total).astype(jnp.bfloat16)
     grad_mix = lax.dot_general(
         grad_in, out_proj, (((1,), (1,)), ((), ())), preferred_element_type=jnp.float32

time: 275 us -> 265 us (0.964)
  waiting for transfers between devices: 95.9 us -> 89.8 us
  matrix products: 44.8 us -> 39.6 us
  other arithmetic: 14 us -> 17 us
    psum x1 -> x0, waiting for transfers between devices: 49.9 us -> none  [on_device(): total = lax.psum(routed.astype(jnp.bfloat16), 'tp').astype(jnp.float32)]
    all_gather x0 -> x1, waiting for transfers between devices: none -> 22.2 us  [on_device(): lax.all_gather(routed.astype(jnp.bfloat16), 'tp')]
    reduce_scatter x1, waiting for transfers between devices: 18.3 us -> 35.7 us  [on_device(): lax.psum_scatter(input_grad(d_gate, d_upper, gate_weight, up_weight).asty...]
    all_to_all x1, waiting for transfers between devices: 0.73 us -> 5.22 us  [on_device(): lax.all_to_all(mine.astype(jnp.bfloat16), 'sp', split_axis=1, concat_axis...]
    reduce_sum x0 -> x1, other arithmetic: none -> 3.07 us  [on_device(): jnp.sum(lax.all_gather(routed.astype(jnp.bfloat16), 'tp'), axis=0)]
where the time goes in v1:
time: 265 us; the launch traced here: 264 us
  waiting for transfers between devices  89.8 us (34%)
  local copies, waits for them, and re-layouts  62.9 us (24%)
  matrix products  39.6 us (15%)
  blocking collectives  35.8 us (14%)
  other arithmetic  17 us (6%)
  between operations  14.4 us (5%)
  starting transfers between devices  4.08 us (2%)
    reduce_scatter x1, waiting for transfers between devices, on_device(): lax.psum_scatter(input_grad(d_gate, d_upper, gate_weight, up_weight).asty...  35.7 us
    all_gather x1, waiting for transfers between devices, on_device(): lax.all_gather(routed.astype(jnp.bfloat16), 'tp')  22.2 us
    all_gather x1, waiting for transfers between devices, on_device(): lax.all_gather(got_cot, 'tp', axis=0, tiled=True)  17.1 us
    all_gather x2, blocking collectives, entering(): everything = jax.tree.map(lambda part: lax.all_gather(part, axis), shard)  17 us
    all_to_all x1, blocking collectives, on_device(): lax.all_to_all(part_in, 'sp', split_axis=1, concat_axis=1, tiled=True)  10.7 us
    reduce_scatter x1, waiting for transfers between devices, on_device(): lax.psum_scatter(lax.dot_general(grad_in, saved_out, (((0,), (0,)), ((),...  9.57 us
    all_to_all x1, blocking collectives, on_device(): lax.all_to_all(part_cot, 'sp', split_axis=1, concat_axis=1, tiled=True)  8.11 us
    mul x3, local copies, waits for them, and re-layouts, on_device(): route_weight[:, :, None] * cotangent[:, None, :].astype(jnp.float32)  7.21 us
  transfers between devices with their start and end apart: 6, of which 5 were waited for; matrix products, arithmetic and copies ran while one was open for 25% of the time, Pallas kernels for 0%

profile of v1, /device:TPU:0, one launch (start us, length us, event | category | flops | bytes accessed | tf_op | source)
XLA Modules:
  0.0 263.9 jit_solution(9186250365814548320)
XLA Ops:
  8.5 1.2 reduce-window.6
  11.3 1.4 scatter_custom_fusion
  12.7 1.9 concatenate.6
  14.6 6.3 %gather_fusion = bf16[512,2048]{1,0:T(8,128)(2,1)} fusion(bf16[129,2048]{1,0:T(8,128)(2,1)} %concatenate.6, s32[1024]{0:T(1024)S(1)} %get-tuple-element.318), kind=kCustom, calls=%fused_computation | custom fusion | bytes 4196352 | tf_op jit(solution)/shard_map/gather | solution.py:198
  21.0 4.1 %reshape.216 = bf16[128,4,2048]{2,1,0:T(4,128)(2,1)} reshape(bf16[512,2048]{1,0:T(8,128)(2,1)} %gather_fusion) | data formatting | bytes 4194304 | tf_op jit(solution)/shard_map/reshape | solution.py:198
  25.1 1.0 constant_dynamic-slice_fusion.1
  26.3 10.7 %all_to_all.15 = bf16[16,4,2048]{2,0,1:T(8,128)(2,1)S(1)} all-to-all(bf16[16,4,2048]{2,0,1:T(8,128)(2,1)S(1)} %copy.182), channel_id=1, replica_groups=mesh['sp'=4,'tp'=8] {'sp'}, dimensions={1} | all-to-all | bytes 524288 | tf_op jit(solution)/shard_map/all_to_all | solution.py:210
  38.0 3.4 %mul.203 = f32[128,2,2048]{2,1,0:T(2,128)} broadcast(bf16[128,2048]{1,0:T(8,128)(2,1)} %param.19), dimensions={0,2} | broadcast | bytes 2621440 | tf_op jit(solution)/shard_map/mul | solution.py:193
  41.4 3.7 %mul.204 = f32[256,2048]{1,0:T(8,128)} reshape(f32[128,2,2048]{2,1,0:T(2,128)} %mul.203) | data formatting | bytes 4194304 | tf_op jit(solution)/shard_map/mul | solution.py:193
  45.3 1.9 multiply_convert_fusion
  47.2 1.1 concatenate.7
  48.3 6.6 %gather_fusion.1 = bf16[512,2048]{1,0:T(8,128)(2,1)} fusion(bf16[257,2048]{1,0:T(8,128)(2,1)} %concatenate.7, s32[1024]{0:T(1024)S(1)} %get-tuple-element.317), kind=kCustom, calls=%fused_computation.1 | custom fusion | bytes 4196352 | tf_op jit(solution)/shard_map/gather | solution.py:201
  54.9 4.1 %reshape.218 = bf16[128,4,2048]{2,1,0:T(4,128)(2,1)} reshape(bf16[512,2048]{1,0:T(8,128)(2,1)} %gather_fusion.1) | data formatting | bytes 4194304 | tf_op jit(solution)/shard_map/reshape | solution.py:201
  59.0 1.0 constant_dynamic-slice_fusion
  60.2 8.1 %all_to_all.16 = bf16[16,4,2048]{2,0,1:T(8,128)(2,1)S(1)} all-to-all(bf16[16,4,2048]{2,0,1:T(8,128)(2,1)S(1)} %copy.183), channel_id=1, replica_groups=mesh['sp'=4,'tp'=8] {'sp'}, dimensions={1} | all-to-all | bytes 524288 | tf_op jit(solution)/shard_map/all_to_all | solution.py:211
  69.5 3.9 %reshape.217 = bf16[512,2048]{1,0:T(8,128)(2,1)} reshape(bf16[128,4,2048]{2,1,0:T(4,128)(2,1)} %all-gather.8.cloned.1.call-done) | data formatting | bytes 4194304 | tf_op jit(solution)/shard_map/reshape | solution.py:218
  73.5 4.7 %fusion.3 = f32[512,768]{1,0:T(8,128)} fusion(bf16[512,2048]{1,0:T(8,128)(2,1)} %reshape.217, bf16[1,2048,768]{2,1,0:T(8,128)(2,1)S(1)} %copy-done), kind=kOutput, calls=%fused_computation.16 | convolution fusion | flops 1610612736 | bytes 6815744 | tf_op jit(solution)/shard_map/dot_general | solution.py:39
  78.2 3.0 %fusion.7 = f32[512,768]{1,0:T(8,128)} fusion(bf16[512,2048]{1,0:T(8,128)(2,1)S(1)} %copy-done.4, bf16[1,2048,768]{2,1,0:T(8,128)(2,1)S(1)} %copy-done.17), kind=kOutput, calls=%fused_computation.20 | convolution fusion | flops 1610612736 | bytes 6815744 | tf_op jit(solution)/shard_map/dot_general | solution.py:40
  81.2 17.1 %all-gather.10.cloned.1.call-done = bf16[128,4,2048]{2,1,0:T(4,128)(2,1)} async-done(((bf16[16,4,2048]{2,1,0:T(4,128)(2,1)}), bf16[128,4,2048]{2,1,0:T(4,128)(2,1)}) %all-gather.10.cloned.1.call-update) | async-done | bytes 2097168 | tf_op jit(solution)/shard_map/all_gather | solution.py:215
  98.3 3.9 %reshape.219 = bf16[512,2048]{1,0:T(8,128)(2,1)} reshape(bf16[128,4,2048]{2,1,0:T(4,128)(2,1)} %all-gather.10.cloned.1.call-done) | data formatting | bytes 4194304 | tf_op jit(solution)/shard_map/reshape | solution.py:218
  102.3 5.6 %multiply_convert_fusion.2 = (bf16[512,768]{1,0:T(8,128)(2,1)S(1)}, bf16[512,768]{1,0:T(8,128)(2,1)S(1)}) fusion(f32[512,768]{1,0:T(8,128)} %fusion.3, f32[512,768]{1,0:T(8,128)} %fusion.7, bf16[512,2048]{1,0:T(8,128)(2,1)} %reshape.219, bf16[1,768,2048]{2,1,0:T(8,128)(2,1)} %param.24), kind=kOutput, calls=%fused_computation.31 | convolution fusion | flops 1615724544 | bytes 9961472 | tf_op jit(solution)/shard_map/dot_general | solution.py:44
  107.9 1.8 fusion.1
  110.4 3.1 %add_convert_fusion = bf16[512,2048]{1,0:T(8,128)(2,1)} fusion(f32[512,2048]{1,0:T(8,128)S(1)} %fusion.1, bf16[512,768]{1,0:T(8,128)(2,1)S(1)} %get-tuple-element.305, bf16[1,2048,768]{2,1,0:T(8,128)(2,1)S(1)} %copy-done.18), kind=kOutput, calls=%fused_computation.10 | convolution fusion | flops 1612709888 | bytes 10223616 | tf_op jit(solution)/shard_map/dot_general | solution.py:67
  113.5 35.7 %reduce-scatter.3.cloned.1.call-done = bf16[64,2048]{1,0:T(8,128)(2,1)} async-done(((bf16[512,2048]{1,0:T(8,128)(2,1)}), bf16[64,2048]{1,0:T(8,128)(2,1)}) %reduce-scatter.3.cloned.1.call-update) | async-done | bytes 262160 | tf_op jit(solution)/shard_map/reduce_scatter | solution.py:221
  149.2 1.1 convert_element_type.114
  151.1 3.7 %all-to-all-start.2 = ((bf16[16,4,2048]{2,0,1:T(8,128)(2,1)}), bf16[16,4,2048]{2,0,1:T(8,128)(2,1)S(1)}, u32[]{:S(2)}, u32[]{:S(2)}) async-start(bf16[16,4,2048]{2,0,1:T(8,128)(2,1)} %copy.151), calls=%async_computation.3 | async-start | bytes 524288 | tf_op jit(solution)/shard_map/all_to_all | solution.py:231
  155.0 5.2 %all-to-all-done.2 = bf16[16,4,2048]{2,0,1:T(8,128)(2,1)S(1)} async-done(((bf16[16,4,2048]{2,0,1:T(8,128)(2,1)}), bf16[16,4,2048]{2,0,1:T(8,128)(2,1)S(1)}, u32[]{:S(2)}, u32[]{:S(2)}) %all-to-all-start.2) | async-done | bytes 262176 | tf_op jit(solution)/shard_map/all_to_all | solution.py:231
  160.6 1.5 gather_fusion.2
  162.1 2.2 gather.14
  164.3 5.7 %select_reduce_fusion = bf16[128,2048]{1,0:T(8,128)(2,1)} fusion(f32[128,2,2048]{2,1,0:T(2,128)} %gather.14, pred[128,2]{1,0:T(8,128)(4,1)S(1)} %copy.150), kind=kLoop, calls=%fused_computation.28 | loop fusion | flops 786432 | bytes 2621696 | tf_op jit(solution)/shard_map/reduce_sum | solution.py:238
  171.1 8.1 %all-gather.3 = f32[4,2,64]{2,1,0:T(2,128)S(1)} all-gather(f32[1,2,64]{2,1,0:T(2,128)S(1)} %exponential_bitcast_fusion.1), channel_id=4, replica_groups=mesh['sp'=4,'tp'=8] {'sp'}, dimensions={0}, use_global_device_ids=true | all-gather | bytes 2560 | tf_op jit(solution)/shard_map/all_gather | solution.py:13
  179.2 1.0 convolution_multiply_fusion.2
  180.2 4.7 %fusion.12 = bf16[1,2048,768]{2,1,0:T(8,128)(2,1)} fusion(bf16[512,2048]{1,0:T(8,128)(2,1)S(1)} %copy-done.5, bf16[512,768]{1,0:T(8,128)(2,1)} %copy-done.19), kind=kOutput, calls=%fused_computation.25 | convolution fusion | flops 1612185600 | bytes 6029312 | tf_op jit(solution)/shard_map/dot_general | solution.py:57
  184.9 3.5 %fusion.11 = bf16[1,2048,768]{2,1,0:T(8,128)(2,1)} fusion(bf16[512,2048]{1,0:T(8,128)(2,1)S(1)} %copy-done.5, bf16[512,768]{1,0:T(8,128)(2,1)S(1)} %copy-done.21), kind=kOutput, calls=%fused_computation.24 | convolution fusion | flops 1612185600 | bytes 6029312 | tf_op jit(solution)/shard_map/dot_general | solution.py:54
  188.5 3.6 %fusion.13 = bf16[1,768,2048]{2,1,0:T(8,128)(2,1)} fusion(bf16[512,2048]{1,0:T(8,128)(2,1)S(1)} %copy-done.6, f32[512,768]{1,0:T(8,128)S(1)} %copy-done.23, f32[512,768]{1,0:T(8,128)S(1)} %copy-done.22), kind=kOutput, calls=%fused_computation.26 | convolution fusion | flops 1614544896 | bytes 8388608 | tf_op jit(solution)/shard_map/dot_general | solution.py:51
  192.0 22.2 %all-gather.12.cloned.1.call-done = bf16[1024,2048]{1,0:T(8,128)(2,1)} async-done(((bf16[128,2048]{1,0:T(8,128)(2,1)}), bf16[1024,2048]{1,0:T(8,128)(2,1)}) %all-gather.12.cloned.1.call-update) | async-done | bytes 4194320 | tf_op jit(solution)/shard_map/all_gather | solution.py:239
  214.2 3.1 %reduce_sum.50 = bf16[128,2048]{1,0:T(8,128)(2,1)S(1)} reduce(bf16[8,128,2048]{2,1,0:T(8,128)(2,1)} %bitcast.121, bf16[]{:T(256)} %constant.131.clone.1), dimensions={0}, to_apply=%region_6.7 | reduce | flops 1835008 | bytes 4718594 | tf_op jit(solution)/shard_map/reduce_sum | solution.py:239
  218.6 8.9 %all-gather.1 = f32[8,64,128]{2,1,0:T(8,128)S(1)} all-gather(f32[2,64,128]{2,1,0:T(8,128)S(1)} %get-tuple-element.245), channel_id=3, replica_groups=mesh['sp'=4,'tp'=8] {'sp'}, dimensions={0}, use_global_device_ids=true | all-gather | bytes 327680 | tf_op jit(solution)/shard_map/all_gather | solution.py:13
  228.1 1.5 convolution_convert_fusion.3
  231.8 1.8 rev.6
  233.6 1.7 copy.175
  235.3 1.3 fusion.24
  236.7 1.0 fusion.57
  238.4 1.7 reshape.230
  240.0 1.4 convolution_multiply_fusion.1
  241.4 1.4 fusion.25
  246.0 9.6 %reduce-scatter.5.cloned.1.call-done = bf16[512,256]{1,0:T(8,128)(2,1)} async-done(((bf16[2048,256]{1,0:T(8,128)(2,1)}), bf16[512,256]{1,0:T(8,128)(2,1)}) %reduce-scatter.5.cloned.1.call-update) | async-done | bytes 262160 | tf_op jit(solution)/shard_map/reduce_scatter | solution.py:244
  255.6 1.8 convert_element_type.120
  (139 shorter events, 17.0 us)
Async XLA Ops:
  7.2 66.3 %copy-start = (bf16[1,2048,768]{2,1,0:T(8,128)(2,1)S(1)}, bf16[1,2048,768]{2,1,0:T(8,128)(2,1)}, u32[]{:S(2)}) copy-start(bf16[1,2048,768]{2,1,0:T(8,128)(2,1)} %param.22) | copy-start | bytes 9437188
  7.2 62.3 %all-gather.8.cloned.1.call-start = ((), (), s32[]{:S(2)}) async-start(), calls=%async_computation.5 | async-start | bytes 2359296 | tf_op jit(solution)/shard_map/all_gather | solution.py:214
  38.0 60.4 %all-gather.10.cloned.1.call-start = ((), (), s32[]{:S(2)}) async-start(), calls=%async_computation.6 | async-start | bytes 2359296 | tf_op jit(solution)/shard_map/all_gather | solution.py:215
  41.4 3.7 %copy-start.16 = (f32[128,2]{0,1:T(2,128)S(1)}, f32[128,2]{0,1:T(2,128)}, u32[]{:S(2)}) copy-start(f32[128,2]{0,1:T(2,128)} %param.21) | copy-start | bytes 3076
  69.3 79.9 %reduce-scatter.3.cloned.1.call-start = ((), (), s32[]{:S(2)}) async-start(), calls=%async_computation.7 | async-start | bytes 2359296 | tf_op jit(solution)/shard_map/reduce_scatter | solution.py:221
  73.5 4.7 %copy-start.4 = (bf16[512,2048]{1,0:T(8,128)(2,1)S(1)}, bf16[512,2048]{1,0:T(8,128)(2,1)}, u32[]{:S(2)}) copy-start(bf16[512,2048]{1,0:T(8,128)(2,1)} %reshape.217) | copy-start | bytes 6291460
  73.5 4.7 %copy-start.17 = (bf16[1,2048,768]{2,1,0:T(8,128)(2,1)S(1)}, bf16[1,2048,768]{2,1,0:T(8,128)(2,1)}, u32[]{:S(2)}) copy-start(bf16[1,2048,768]{2,1,0:T(8,128)(2,1)} %param.23) | copy-start | bytes 9437188
  107.9 1.9 copy-start.20
  107.9 1.9 copy-start.19
  107.9 2.5 copy-start.18
  151.1 9.1 %all-to-all-start.2 = ((bf16[16,4,2048]{2,0,1:T(8,128)(2,1)}), bf16[16,4,2048]{2,0,1:T(8,128)(2,1)S(1)}, u32[]{:S(2)}, u32[]{:S(2)}) async-start(bf16[16,4,2048]{2,0,1:T(8,128)(2,1)} %copy.151), calls=%async_computation.3 | async-start | bytes 524288 | tf_op jit(solution)/shard_map/all_to_all | solution.py:231
  154.8 59.4 %all-gather.12.cloned.1.call-start = ((), (), s32[]{:S(2)}) async-start(), calls=%async_computation.9 | async-start | bytes 4718592 | tf_op jit(solution)/shard_map/all_gather | solution.py:239
  164.3 5.9 %copy-start.11 = (f32[128,128]{1,0:T(8,128)S(1)}, f32[128,128]{1,0:T(8,128)}, u32[]{:S(2)}) copy-start(f32[128,128]{1,0:T(8,128)} %param.30) | copy-start | bytes 196612
  164.3 6.2 %copy-start.14 = (bf16[128,128]{1,0:T(8,128)(2,1)S(1)}, bf16[128,128]{1,0:T(8,128)(2,1)}, u32[]{:S(2)}) copy-start(bf16[128,128]{1,0:T(8,128)(2,1)} %param.27) | copy-start | bytes 98308
  164.3 6.4 %copy-start.15 = (bf16[128,128]{1,0:T(8,128)(2,1)S(1)}, bf16[128,128]{1,0:T(8,128)(2,1)}, u32[]{:S(2)}) copy-start(bf16[128,128]{1,0:T(8,128)(2,1)} %param.28) | copy-start | bytes 98308
  164.3 6.7 %copy-start.13 = (bf16[128,256]{1,0:T(8,128)(2,1)S(1)}, bf16[128,256]{1,0:T(8,128)(2,1)}, u32[]{:S(2)}) copy-start(bf16[128,256]{1,0:T(8,128)(2,1)} %param.29) | copy-start | bytes 196612
  170.1 10.1 %copy-start.5 = (bf16[512,2048]{1,0:T(8,128)(2,1)S(1)}, bf16[512,2048]{1,0:T(8,128)(2,1)}, u32[]{:S(2)}) copy-start(bf16[512,2048]{1,0:T(8,128)(2,1)} %reshape.217) | copy-start | bytes 6291460
  170.1 85.5 %reduce-scatter.5.cloned.1.call-start = ((), (), s32[]{:S(2)}) async-start(), calls=%async_computation.8 | async-start | bytes 1310720 | tf_op jit(solution)/shard_map/reduce_scatter | solution.py:244
  180.2 4.7 %copy-start.21 = (bf16[512,768]{1,0:T(8,128)(2,1)S(1)}, bf16[512,768]{1,0:T(8,128)(2,1)}, u32[]{:S(2)}) copy-start(bf16[512,768]{1,0:T(8,128)(2,1)} %copy-done.20) | copy-start | bytes 2359300
  184.9 3.5 %copy-start.6 = (bf16[512,2048]{1,0:T(8,128)(2,1)S(1)}, bf16[512,2048]{1,0:T(8,128)(2,1)}, u32[]{:S(2)}) copy-start(bf16[512,2048]{1,0:T(8,128)(2,1)} %reshape.219) | copy-start | bytes 6291460
  184.9 3.5 %copy-start.22 = (f32[512,768]{1,0:T(8,128)S(1)}, f32[512,768]{1,0:T(8,128)}, u32[]{:S(2)}) copy-start(f32[512,768]{1,0:T(8,128)} %fusion.3) | copy-start | bytes 4718596
  184.9 3.5 %copy-start.23 = (f32[512,768]{1,0:T(8,128)S(1)}, f32[512,768]{1,0:T(8,128)}, u32[]{:S(2)}) copy-start(f32[512,768]{1,0:T(8,128)} %fusion.7) | copy-start | bytes 4718596
  214.2 3.1 %copy-start.2 = (bf16[128,2048]{1,0:T(8,128)(2,1)S(1)}, bf16[128,2048]{1,0:T(8,128)(2,1)}, u32[]{:S(2)}) copy-start(bf16[128,2048]{1,0:T(8,128)(2,1)} %param.19) | copy-start | bytes 1572868
  214.2 3.1 %copy-start.8 = (bf16[256,2048]{1,0:T(8,128)(2,1)S(1)}, bf16[256,2048]{1,0:T(8,128)(2,1)}, u32[]{:S(2)}) copy-start(bf16[256,2048]{1,0:T(8,128)(2,1)} %param.25) | copy-start | bytes 3145732
  217.8 10.3 %copy-start.12 = (bf16[128,256]{1,0:T(8,128)(2,1)S(1)}, bf16[128,256]{1,0:T(8,128)(2,1)}, u32[]{:S(2)}) copy-start(bf16[128,256]{1,0:T(8,128)(2,1)} %param.26) | copy-start | bytes 196612
  217.9 11.9 %copy-start.3 = (f32[2,64,2,128]{3,2,1,0:T(2,128)}, f32[2,64,2,128]{3,2,1,0:T(2,128)S(1)}, u32[]{:S(2)}) copy-start(f32[2,64,2,128]{3,2,1,0:T(2,128)S(1)} %reshape.225) | copy-start | bytes 393220
  218.5 11.6 %copy-start.7 = (f32[2,2,64,128]{3,2,1,0:T(8,128)}, f32[2,2,64,128]{3,2,1,0:T(8,128)S(1)}, u32[]{:S(2)}) copy-start(f32[2,2,64,128]{3,2,1,0:T(8,128)S(1)} %get-tuple-element.244) | copy-start | bytes 393220
  228.1 1.7 copy-start.9
  231.8 25.5 %copy-start.1 = (bf16[1,2048,768]{2,1,0:T(8,128)(2,1)S(1)}, bf16[1,2048,768]{2,1,0:T(8,128)(2,1)}, u32[]{:S(2)}) copy-start(bf16[1,2048,768]{2,1,0:T(8,128)(2,1)} %param.22) | copy-start | bytes 9437188
  236.6 8.5 %copy-start.10 = (bf16[2,64,2,64]{1,3,2,0:T(8,128)(2,1)S(1)}, bf16[2,64,2,64]{1,3,2,0:T(8,128)(2,1)}, u32[]{:S(2)}) copy-start(bf16[2,64,2,64]{1,3,2,0:T(8,128)(2,1)} %get-tuple-element.309) | copy-start | bytes 98308
Sparse Core Ops, SparseCore 0:
  38.1 28.8 all-gather.7
  69.4 28.8 all-gather.9
  113.7 35.4 reduce-scatter.2
  170.2 43.9 all-gather.11
  229.7 25.8 reduce-scatter.4
